TPU v7x, 32 devices: a whole 2x2x4 slice. The times are simulated.
32 devices in a mesh: dp: 4 (over y, x), kv: 4 (over z), tp: 2 (over core).
Axes of the slice: x: 2, y: 2, z: 4, core: 2. Of those that a mesh axis runs over, the one named last changes fastest.
Arguments:
- resid: bfloat16 [16, 2048], P('dp', ('kv', 'tp')), may hold values from -45 to 45
- norm_gain: bfloat16 [3, 2048], P(None, ('kv', 'tp')), may hold values from 0.099609375 to 1.8984375
- ffn_gate: bfloat16 [2, 2048, 5632], P(None, None, ('kv', 'tp')), may hold values from -0.125 to 0.125
- ffn_up: bfloat16 [2, 2048, 5632], P(None, None, ('kv', 'tp')), may hold values from -0.125 to 0.125
- ffn_down: bfloat16 [2, 5632, 2048], P(None, ('kv', 'tp')), may hold values from -0.109375 to 0.109375
- w_x: bfloat16 [2048, 64, 64], P(None, 'kv', 'tp'), may hold values from -0.125 to 0.125
- w_z: bfloat16 [2048, 64, 64], P(None, 'kv', 'tp'), may hold values from -0.125 to 0.125
- w_bc: bfloat16 [2048, 2, 8, 128], P('kv'), may hold values from -0.125 to 0.125
- w_dt: bfloat16 [2048, 64], P('kv'), may hold values from -0.125 to 0.125
- dt_bias: float32 [64], replicated, may hold values from -2 to 0.5
- a_log: float32 [64], replicated, may hold values from -1.5 to 1.5
- d_skip: float32 [64], replicated, may hold values from 0.5 to 1.5
- conv_wx: bfloat16 [4, 64, 64], P(None, None, 'tp'), may hold values from -3 to 3
- conv_wbc: bfloat16 [4, 2, 8, 128], replicated, may hold values from -3 to 3
- conv_x: bfloat16 [16, 3, 64, 64], P(('dp', 'kv'), None, None, 'tp'), may hold values from -6 to 6
- conv_bc: bfloat16 [16, 3, 2, 8, 128], P(('dp', 'kv')), may hold values from -6 to 6
- ssm_state: float32 [16, 64, 64, 128], P(('dp', 'kv'), None, 'tp'), may hold values from -3 to 3
- w_out: bfloat16 [64, 64, 2048], P(None, 'tp', 'kv'), may hold values from -0.09375 to 0.09375
Outputs:
- final: bfloat16 [16, 2048], P('dp', ('kv', 'tp'))
All inputs are finite; a program needn't handle non-finite values.
Results may differ from a plain program's by a relative error of at most 0.018.
Values may be sent and summed in bfloat16 or wider, within the bound.
No kernel may reach another device: no remote copies, remote signals or barrier semaphores. Data moves between devices by JAX's collectives and lax.ppermute only.
A program may use at most 64 MiB of HBM per device.

v0:
```python
import jax
import jax.numpy as jnp
from jax import lax
from jax.sharding import PartitionSpec as P

D = 2048
EPS = 1e-06


def normalize(rows, gain):
    values = rows.astype(jnp.float32)
    scale = lax.rsqrt(jnp.mean(values * values, axis=1, keepdims=True) + EPS)
    return (values * scale * gain.astype(jnp.float32).reshape(1, -1)).astype(jnp.bfloat16)


def feed_forward(normed, w_gate, w_up, w_down):
    gate = jnp.dot(normed, w_gate, preferred_element_type=jnp.float32)
    upper = jnp.dot(normed, w_up, preferred_element_type=jnp.float32)
    hidden = (jax.nn.silu(gate) * upper).astype(jnp.bfloat16)
    return jnp.dot(hidden, w_down, preferred_element_type=jnp.float32)


def add_half(base, sums):
    return (base.astype(jnp.float32) + 0.5 * sums).astype(jnp.bfloat16)


def ffn_totals(partial_value):
    return lax.psum(partial_value, ("kv", "tp"))


def short_conv(history, newest, taps):
    window = jnp.concatenate(
        [history.astype(jnp.float32), newest.astype(jnp.float32)[:, None]], axis=1
    )
    return jax.nn.silu(jnp.sum(window * taps.astype(jnp.float32)[None], axis=1))


def state_step(
    xs_new,
    zeta,
    bc_new,
    dt_raw,
    conv_x,
    conv_bc,
    ssm_state,
    conv_wx,
    conv_wbc,
    dt_bias,
    a_log,
    d_skip,
):
    xconv = short_conv(conv_x, xs_new, conv_wx)
    bconv = short_conv(conv_bc, bc_new, conv_wbc)
    heads = xconv.shape[1]
    groups = bconv.shape[2]
    bmat = jnp.repeat(bconv[:, 0], heads // groups, axis=1)
    cmat = jnp.repeat(bconv[:, 1], heads // groups, axis=1)
    step_size = jax.nn.softplus(dt_raw + dt_bias[None, :])
    decay = jnp.exp(-step_size * jnp.exp(a_log)[None, :])
    updated = (
        decay[:, :, None, None] * ssm_state
        + (step_size[:, :, None] * xconv)[..., None] * bmat[:, :, None, :]
    )
    mixed = (
        jnp.einsum("shpn,shn->shp", updated, cmat, precision=lax.Precision.HIGHEST)
        + d_skip[None, :, None] * xconv
    )
    return (mixed * jax.nn.silu(zeta.astype(jnp.float32))).astype(jnp.bfloat16)


def group_terms(slab, w_bc, w_dt):
    span = slab.shape[1]
    flat_bc = w_bc.reshape(span, -1)
    bc_part = jnp.dot(slab, flat_bc, preferred_element_type=jnp.float32)
    dt_part = jnp.dot(slab, w_dt, preferred_element_type=jnp.float32)
    return (
        lax.psum_scatter(bc_part, "kv", scatter_dimension=0, tiled=True),
        lax.psum_scatter(dt_part, "kv", scatter_dimension=0, tiled=True),
    )


def mix_partial(
    normed,
    w_x,
    w_z,
    w_bc,
    w_dt,
    dt_bias,
    a_log,
    d_skip,
    conv_wx,
    conv_wbc,
    conv_x,
    conv_bc,
    ssm_state,
    w_out,
):
    rows = normed.shape[0]
    local_heads = w_x.shape[1]
    half = w_x.shape[2]
    xs_part = (
        jnp.dot(normed, w_x.reshape(D, -1), preferred_element_type=jnp.float32)
        .astype(jnp.bfloat16)
        .reshape(rows, local_heads, half)
    )
    zeta_part = (
        jnp.dot(normed, w_z.reshape(D, -1), preferred_element_type=jnp.float32)
        .astype(jnp.bfloat16)
        .reshape(rows, local_heads, half)
    )
    xs_new, zeta = (
        lax.all_to_all(xs_part, "kv", split_axis=0, concat_axis=1, tiled=True),
        lax.all_to_all(zeta_part, "kv", split_axis=0, concat_axis=1, tiled=True),
    )
    span = w_bc.shape[0]
    slab = lax.dynamic_slice_in_dim(normed, lax.axis_index("kv") * span, span, 1)
    bc_sum, dt_raw = group_terms(slab, w_bc, w_dt)
    bc_new = bc_sum.astype(jnp.bfloat16).reshape((bc_sum.shape[0],) + w_bc.shape[1:])
    mixed = state_step(
        xs_new,
        zeta,
        bc_new,
        dt_raw,
        conv_x,
        conv_bc,
        ssm_state,
        conv_wx,
        conv_wbc,
        dt_bias,
        a_log,
        d_skip,
    )
    flat_out = w_out.reshape(-1, w_out.shape[2])
    piece = lax.all_gather(mixed, "kv", axis=0, tiled=True)
    return jnp.dot(piece.reshape(piece.shape[0], -1), flat_out, preferred_element_type=jnp.float32)


def per_device(
    resid,
    norm_gain,
    ffn_gate,
    ffn_up,
    ffn_down,
    w_x,
    w_z,
    w_bc,
    w_dt,
    dt_bias,
    a_log,
    d_skip,
    conv_wx,
    conv_wbc,
    conv_x,
    conv_bc,
    ssm_state,
    w_out,
):
    mixer_args = (
        w_x,
        w_z,
        w_bc,
        w_dt,
        dt_bias,
        a_log,
        d_skip,
        conv_wx,
        conv_wbc,
        conv_x,
        conv_bc,
        ssm_state,
        w_out,
    )
    rows, gains = (
        lax.all_gather(resid, ("kv", "tp"), axis=1, tiled=True),
        lax.all_gather(norm_gain, ("kv", "tp"), axis=1, tiled=True),
    )
    first = add_half(
        rows,
        ffn_totals(feed_forward(normalize(rows, gains[0]), ffn_gate[0], ffn_up[0], ffn_down[0])),
    )
    partial_value = mix_partial(normalize(first, gains[1]), *mixer_args)
    span = partial_value.shape[1]
    block = lax.dynamic_slice_in_dim(first, lax.axis_index("kv") * span, span, 1)
    joined = (block.astype(jnp.float32) + lax.psum(partial_value, "tp")).astype(jnp.bfloat16)
    second = lax.all_gather(joined, "kv", axis=1, tiled=True)
    final = add_half(
        second,
        ffn_totals(feed_forward(normalize(second, gains[2]), ffn_gate[1], ffn_up[1], ffn_down[1])),
    )
    width = resid.shape[1]
    return lax.dynamic_slice_in_dim(final, lax.axis_index(("kv", "tp")) * width, width, 1)


def solution(mesh):
    placed = (
        P("dp", ("kv", "tp")),
        P(None, ("kv", "tp")),
        P(None, None, ("kv", "tp")),
        P(None, None, ("kv", "tp")),
        P(None, ("kv", "tp"), None),
        P(None, "kv", "tp"),
        P(None, "kv", "tp"),
        P("kv", None, None, None),
        P("kv", None),
        P(),
        P(),
        P(),
        P(None, None, "tp"),
        P(),
        P(("dp", "kv"), None, None, "tp"),
        P(("dp", "kv"), None, None, None, None),
        P(("dp", "kv"), None, "tp", None),
        P(None, "tp", "kv"),
    )
    return jax.shard_map(
        per_device, mesh=mesh, in_specs=placed, out_specs=P("dp", ("kv", "tp")), check_vma=False
    )
```

profile of v0, /device:TPU:0, one launch (start us, length us, event | category | flops | bytes accessed | tf_op | source)
XLA Modules:
  0.0 168.5 jit_solution(16530086735748407296)
XLA Ops:
  0.0 14.7 %all_gather.12 = bf16[4,2048]{1,0:T(4,128)(2,1)S(1)} all-gather(bf16[4,256]{1,0:T(4,128)(2,1)} %param.18), channel_id=1, replica_groups=mesh['dp'=4,'kv'=4,'tp'=2] {'kv','tp'}, dimensions={1}, use_global_device_ids=true | all-gather | bytes 18432 | tf_op jit(solution)/shard_map/all_gather | solution.py:174
  14.7 0.1 fusion.48
  14.9 12.9 %all_gather.13 = bf16[3,2048]{1,0:T(4,128)(2,1)S(1)} all-gather(bf16[3,256]{1,0:T(4,128)(2,1)} %param.19), channel_id=1, replica_groups=mesh['dp'=4,'kv'=4,'tp'=2] {'kv','tp'}, dimensions={1}, use_global_device_ids=true | all-gather | bytes 13824 | tf_op jit(solution)/shard_map/all_gather | solution.py:175
  27.8 2.7 %fusion.10 = f32[4,704]{1,0:T(4,128)S(1)} fusion(bf16[2,2048,704]{1,2,0:T(8,128)(2,1)} %param.20, bf16[4,2048]{1,0:T(4,128)(2,1)S(1)} %all_gather.12, f32[2048]{0:T(1024)S(1)} %bitcast.113, f32[4]{0:T(128)S(1)} %add_rsqrt_fusion.2), kind=kOutput, calls=%fused_computation.10 | convolution fusion | flops 11567104 | bytes 2919440 | tf_op jit(solution)/shard_map/dot_general | solution.py:17
  30.5 4.4 %fusion.6 = f32[4,2048]{1,0:T(4,128)S(1)} fusion(bf16[2,704,2048]{2,1,0:T(8,128)(2,1)} %param.22, bf16[2,2048,704]{1,2,0:T(8,128)(2,1)} %param.21, f32[4,704]{1,0:T(4,128)S(1)} %fusion.10, bf16[4,2048]{1,0:T(4,128)(2,1)S(1)} %all_gather.12, f32[2048]{0:T(1024)S(1)} %bitcast.114, f32[4]{0:T(128)S(1)} %add_rsqrt_fusion.2), kind=kOutput, calls=%fused_computation.6 | convolution fusion | flops 23118336 | bytes 5835792 | tf_op jit(solution)/shard_map/dot_general | solution.py:20
  34.8 26.7 %psum.21 = f32[4,2048]{1,0:T(4,128)S(1)} all-reduce(f32[4,2048]{1,0:T(4,128)S(1)} %fusion.6), channel_id=1, replica_groups=mesh['dp'=4,'kv'=4,'tp'=2] {'kv','tp'}, use_global_device_ids=true, to_apply=%region_1.2 | all-reduce | flops 8192 | bytes 65536 | tf_op jit(solution)/shard_map/psum | solution.py:28
  61.5 0.1 fusion.45
  61.6 0.1 fusion.47
  61.7 0.0 copy-start.10
  61.7 0.0 copy-start.5
  61.8 0.0 copy-start.6
  61.8 0.0 copy-start.8
  61.8 0.0 copy-start.9
  61.8 0.6 convolution_convert_fusion.1
  62.4 0.0 copy-start.1
  62.5 0.1 reshape.198
  62.5 0.7 reshape.219
  63.2 3.2 %all-to-all-start = ((bf16[4,2,256]{2,1,0:T(2,128)(2,1)}), bf16[4,2,256]{2,1,0:T(2,128)(2,1)S(1)}, u32[]{:S(2)}, u32[]{:S(2)}) async-start(bf16[4,2,256]{2,1,0:T(2,128)(2,1)} %reshape.219), calls=%async_computation | async-start | bytes 8192 | tf_op jit(solution)/shard_map/all_to_all | solution.py:112
  66.5 0.0 copy-start.7
  66.5 2.2 %convolution_convert_fusion = bf16[4,512]{1,0:T(4,128)(2,1)S(1)} fusion(bf16[4,2048]{1,0:T(4,128)(2,1)S(1)} %fusion.47, bf16[2048,512]{0,1:T(8,128)(2,1)} %bitcast.109), kind=kOutput, calls=%fused_computation.26 | convolution fusion | flops 8390656 | bytes 2117632 | tf_op jit(solution)/shard_map/dot_general | solution.py:107
  68.7 0.1 fusion.69
  68.9 2.0 %fusion.18 = f32[4,2048]{1,0:T(4,128)S(1)} fusion(bf16[64,8,16,128]{3,2,1,0:T(8,128)(2,1)} %bitcast.108, bf16[4,2048]{1,0:T(4,128)(2,1)S(1)} %fusion.47, s32[]{:T(128)S(6)} %select_n.11), kind=kOutput, calls=%fused_computation.18 | convolution fusion | flops 8388608 | bytes 2134020 | tf_op jit(solution)/shard_map/dot_general | solution.py:74
  70.9 0.6 dynamic-slice
  71.4 19.8 %all-reduce.2 = (bf16[4,2048]{1,0:T(4,128)(2,1)S(1)}, f32[4,64]{1,0:T(4,128)S(1)}) all-reduce(f32[4,2048]{1,0:T(4,128)S(1)} %fusion.18, f32[4,64]{1,0:T(4,128)S(1)} %fusion.69), channel_id=4, replica_groups=mesh['dp'=4,'kv'=4,'tp'=2] {'kv'}, use_global_device_ids=true, to_apply=%region_5.6.clone | all-reduce | flops 8448 | bytes 51200
  91.2 0.7 fusion.60
  92.0 0.1 reshape.202
  92.1 0.7 reshape.217
  92.7 0.0 all-to-all-done
  92.8 3.2 %all-to-all-start.1 = ((bf16[4,2,256]{2,1,0:T(2,128)(2,1)}), bf16[4,2,256]{2,1,0:T(2,128)(2,1)S(1)}, u32[]{:S(2)}, u32[]{:S(2)}) async-start(bf16[4,2,256]{2,1,0:T(2,128)(2,1)} %reshape.217), calls=%async_computation.1 | async-start | bytes 8192 | tf_op jit(solution)/shard_map/all_to_all | solution.py:113
  96.0 0.7 fusion.75
  96.7 0.1 reshape.220
  96.8 0.1 copy.27
  96.9 4.7 %all-to-all-done.1 = bf16[4,2,256]{2,1,0:T(2,128)(2,1)S(1)} async-done(((bf16[4,2,256]{2,1,0:T(2,128)(2,1)}), bf16[4,2,256]{2,1,0:T(2,128)(2,1)S(1)}, u32[]{:S(2)}, u32[]{:S(2)}) %all-to-all-start.1) | async-done | bytes 4128 | tf_op jit(solution)/shard_map/all_to_all | solution.py:113
  101.6 0.1 reshape.218
  101.7 0.1 copy.30
  101.8 0.1 copy.28
  101.9 1.9 %fusion.33 = f32[64,1,32]{2,1,0:T(1,128)S(1)} fusion(f32[64,128,1]{1,2,0:T(1,128)S(1)} %bitcast.110, f32[1,64,32,128]{3,2,1,0:T(8,128)S(1)} %copy-done.1, f32[64,128]{1,0:T(8,128)S(1)} %broadcast_bitcast_fusion, f32[64,32]{1,0:T(8,128)S(1)} %copy.28, f32[64]{0:T(128)S(1)} %get-tuple-element.7), kind=kOutput, calls=%fused_computation.28 | convolution fusion | flops 3932160 | bytes 1130752 | tf_op jit(solution)/shard_map/shpn,shn->shp/dot_general | solution.py:65
  103.8 0.1 copy.34
  103.9 13.1 %all-gather.1 = bf16[4,64,32]{1,2,0:T(8,128)(2,1)S(1)} all-gather(bf16[1,64,32]{1,2,0:T(8,128)(2,1)S(1)} %fusion.64), channel_id=2, replica_groups=mesh['dp'=4,'kv'=4,'tp'=2] {'kv'}, dimensions={0}, use_global_device_ids=true | all-gather | bytes 20480 | tf_op jit(solution)/shard_map/all_gather | solution.py:134
  117.0 0.1 copy.35
  117.1 2.0 %convolution_bitcast_fusion = f32[4,512]{1,0:T(4,128)S(1)} fusion(bf16[4,64,32]{2,0,1:T(4,128)(2,1)S(1)} %copy.35, bf16[64,32,512]{2,1,0:T(8,128)(2,1)} %param.35), kind=kOutput, calls=%fused_computation.25 | convolution fusion | flops 8388608 | bytes 2121728 | tf_op jit(solution)/shard_map/dot_general | solution.py:135
  119.2 2.5 %psum.22 = f32[4,512]{1,0:T(4,128)S(1)} all-reduce(f32[4,512]{1,0:T(4,128)S(1)} %convolution_bitcast_fusion), channel_id=1, replica_groups=mesh['dp'=4,'kv'=4,'tp'=2] {'tp'}, use_global_device_ids=true, to_apply=%region_7.8 | all-reduce | flops 2048 | bytes 16384 | tf_op jit(solution)/shard_map/psum | solution.py:184
  121.6 13.2 %all_gather.15 = bf16[4,2048]{1,0:T(4,128)(2,1)S(1)} all-gather(bf16[4,512]{1,0:T(4,128)(2,1)S(1)} %add_convert_fusion), channel_id=1, replica_groups=mesh['dp'=4,'kv'=4,'tp'=2] {'kv'}, dimensions={1}, use_global_device_ids=true | all-gather | bytes 20480 | tf_op jit(solution)/shard_map/all_gather | solution.py:185
  134.8 0.1 multiply_reduce_fusion.1
  135.0 2.7 %fusion.4 = f32[4,704]{1,0:T(4,128)S(1)} fusion(bf16[2,2048,704]{1,2,0:T(8,128)(2,1)} %param.20, f32[2048]{0:T(1024)S(1)} %bitcast.111, f32[4]{0:T(128)S(1)} %add_rsqrt_fusion, bf16[4,2048]{1,0:T(4,128)(2,1)S(1)} %all_gather.15), kind=kOutput, calls=%fused_computation.4 | convolution fusion | flops 11567104 | bytes 2919440 | tf_op jit(solution)/shard_map/dot_general | solution.py:17
  137.7 4.4 %fusion = f32[4,2048]{1,0:T(4,128)S(1)} fusion(bf16[2,704,2048]{2,1,0:T(8,128)(2,1)} %param.22, bf16[2,2048,704]{1,2,0:T(8,128)(2,1)} %param.21, f32[4,704]{1,0:T(4,128)S(1)} %fusion.4, f32[2048]{0:T(1024)S(1)} %bitcast.112, f32[4]{0:T(128)S(1)} %add_rsqrt_fusion, bf16[4,2048]{1,0:T(4,128)(2,1)S(1)} %all_gather.15), kind=kOutput, calls=%fused_computation | convolution fusion | flops 23118336 | bytes 5835792 | tf_op jit(solution)/shard_map/dot_general | solution.py:20
  142.0 25.9 %psum.23 = f32[4,2048]{1,0:T(4,128)S(1)} all-reduce(f32[4,2048]{1,0:T(4,128)S(1)} %fusion), channel_id=1, replica_groups=mesh['dp'=4,'kv'=4,'tp'=2] {'kv','tp'}, use_global_device_ids=true, to_apply=%region_9.10 | all-reduce | flops 8192 | bytes 65536 | tf_op jit(solution)/shard_map/psum | solution.py:28
  168.0 0.6 fusion.67
  (30 shorter events, 0.2 us)
Async XLA Ops:
  0.0 61.7 %copy-start = (bf16[2048,16,32]{0,2,1:T(8,128)(2,1)S(1)}, bf16[2048,16,32]{0,2,1:T(8,128)(2,1)}, u32[]{:S(2)}) copy-start(bf16[2048,16,32]{0,2,1:T(8,128)(2,1)} %param.23) | copy-start | bytes 6291460
  34.8 33.9 %copy-start.2 = (bf16[512,64]{0,1:T(8,128)(2,1)S(1)}, bf16[512,64]{0,1:T(8,128)(2,1)}, u32[]{:S(2)}) copy-start(bf16[512,64]{0,1:T(8,128)(2,1)} %param.26) | copy-start | bytes 196612
  61.7 9.1 %copy-start.10 = (u32[32]{0:T(128)S(1)}, u32[32]{0:T(128)}, u32[]{:S(2)}) copy-start(u32[32]{0:T(128)} %constant.45) | copy-start | bytes 388
  61.7 30.2 %copy-start.5 = (bf16[4,2,8,128]{3,2,1,0:T(8,128)(2,1)S(1)}, bf16[4,2,8,128]{3,2,1,0:T(8,128)(2,1)}, u32[]{:S(2)}) copy-start(bf16[4,2,8,128]{3,2,1,0:T(8,128)(2,1)} %param.31) | copy-start | bytes 49156
  61.8 30.2 %copy-start.6 = (bf16[1,3,2,8,128]{4,3,2,1,0:T(8,128)(2,1)S(1)}, bf16[1,3,2,8,128]{4,3,2,1,0:T(8,128)(2,1)}, u32[]{:S(2)}) copy-start(bf16[1,3,2,8,128]{4,3,2,1,0:T(8,128)(2,1)} %param.33) | copy-start | bytes 36868
  61.8 34.2 %copy-start.8 = (f32[64]{0:T(128)S(1)}, f32[64]{0:T(128)}, u32[]{:S(2)}) copy-start(f32[64]{0:T(128)} %param.28) | copy-start | bytes 772
  61.8 34.2 %copy-start.9 = (f32[64]{0:T(128)S(1)}, f32[64]{0:T(128)}, u32[]{:S(2)}) copy-start(f32[64]{0:T(128)} %param.27) | copy-start | bytes 772
  62.4 39.3 %copy-start.3 = (bf16[4,64,32]{1,2,0:T(8,128)(2,1)S(1)}, bf16[4,64,32]{1,2,0:T(8,128)(2,1)}, u32[]{:S(2)}) copy-start(bf16[4,64,32]{1,2,0:T(8,128)(2,1)} %param.30) | copy-start | bytes 49156
  62.4 39.3 %copy-start.4 = (bf16[1,3,64,32]{2,3,1,0:T(8,128)(2,1)S(1)}, bf16[1,3,64,32]{2,3,1,0:T(8,128)(2,1)}, u32[]{:S(2)}) copy-start(bf16[1,3,64,32]{2,3,1,0:T(8,128)(2,1)} %param.32) | copy-start | bytes 36868
  62.4 39.4 %copy-start.1 = (f32[1,64,32,128]{3,2,1,0:T(8,128)S(1)}, f32[1,64,32,128]{3,2,1,0:T(8,128)}, u32[]{:S(2)}) copy-start(f32[1,64,32,128]{3,2,1,0:T(8,128)} %param.34) | copy-start | bytes 3145732
  63.2 29.5 %all-to-all-start = ((bf16[4,2,256]{2,1,0:T(2,128)(2,1)}), bf16[4,2,256]{2,1,0:T(2,128)(2,1)S(1)}, u32[]{:S(2)}, u32[]{:S(2)}) async-start(bf16[4,2,256]{2,1,0:T(2,128)(2,1)} %reshape.219), calls=%async_computation | async-start | bytes 8192 | tf_op jit(solution)/shard_map/all_to_all | solution.py:112
  66.5 37.4 %copy-start.7 = (f32[64]{0:T(128)S(1)}, f32[64]{0:T(128)}, u32[]{:S(2)}) copy-start(f32[64]{0:T(128)} %param.29) | copy-start | bytes 772
  92.8 8.8 %all-to-all-start.1 = ((bf16[4,2,256]{2,1,0:T(2,128)(2,1)}), bf16[4,2,256]{2,1,0:T(2,128)(2,1)S(1)}, u32[]{:S(2)}, u32[]{:S(2)}) async-start(bf16[4,2,256]{2,1,0:T(2,128)(2,1)} %reshape.217), calls=%async_computation.1 | async-start | bytes 8192 | tf_op jit(solution)/shard_map/all_to_all | solution.py:113
where the time goes:
time: 169 us
  blocking collectives  129 us (76%)
  matrix products  22.9 us (14%)
  starting transfers between devices  6.47 us (4%)
  waiting for transfers between devices  4.68 us (3%)
  local copies, waits for them, and re-layouts  3.47 us (2%)
  other arithmetic  1.89 us (1%)
    psum x2, blocking collectives, ffn_totals(): return lax.psum(partial_value, ('kv', 'tp'))  52.6 us
    unnamed x1, blocking collectives  19.8 us
    all_gather x1, blocking collectives, per_device(): lax.all_gather(resid, ('kv', 'tp'), axis=1, tiled=True)  14.7 us
    all_gather x1, blocking collectives, per_device(): second = lax.all_gather(joined, 'kv', axis=1, tiled=True)  13.2 us
    all_gather x1, blocking collectives, mix_partial(): piece = lax.all_gather(mixed, 'kv', axis=0, tiled=True)  13.1 us
    all_gather x1, blocking collectives, per_device(): lax.all_gather(norm_gain, ('kv', 'tp'), axis=1, tiled=True)  12.9 us
    dot_general x2, matrix products, feed_forward(): return jnp.dot(hidden, w_down, preferred_element_type=jnp.float32)  8.72 us
    dot_general x2, matrix products, feed_forward(): gate = jnp.dot(normed, w_gate, preferred_element_type=jnp.float32)  5.31 us
  transfers between devices with their start and end apart: 2, of which 1 were waited for; matrix products, arithmetic and copies ran while one was open for 4% of the time, Pallas kernels for 0%

commit v1 on v0

--- a/solution.py
+++ b/solution.py
@@ -5,6 +5,11 @@
 
 D = 2048
 EPS = 1e-06
+
+
+def build_circles(field_in):
+    all_rows = jnp.sum(lax.all_gather(field_in, ("kv", "tp")), 0)
+    return all_rows
 
 
 def normalize(rows, gain):
@@ -25,7 +30,7 @@
 
 
 def ffn_totals(partial_value):
-    return lax.psum(partial_value, ("kv", "tp"))
+    return build_circles(partial_value)
 
 
 def short_conv(history, newest, taps):

time: 169 us -> 144 us (0.85)
  blocking collectives: 129 us -> 105 us
    psum x2 -> x0, blocking collectives: 52.6 us -> none  [ffn_totals(): return lax.psum(partial_value, ('kv', 'tp'))]
    all_gather x0 -> x2, blocking collectives: none -> 28.5 us  [build_circles(): all_rows = jnp.sum(lax.all_gather(field_in, ('kv', 'tp')), 0)]
  transfers between devices with their start and end apart: 2 -> 2, of which waited for: 1 -> 1; matrix products, arithmetic and copies ran while one was open for 4% -> 7% of each run, Pallas kernels for 0% -> 0%
where the time goes in v1:
time: 144 us; the launch traced here: 143 us
  blocking collectives  105 us (73%)
  matrix products  22.9 us (16%)
  starting transfers between devices  6.47 us (4%)
  local copies, waits for them, and re-layouts  3.49 us (2%)
  waiting for transfers between devices  3.27 us (2%)
  other arithmetic  1.99 us (1%)
    all_gather x2, blocking collectives, build_circles(): all_rows = jnp.sum(lax.all_gather(field_in, ('kv', 'tp')), 0)  28.5 us
    unnamed x1, blocking collectives  19.8 us
    all_gather x1, blocking collectives, per_device(): lax.all_gather(resid, ('kv', 'tp'), axis=1, tiled=True)  14.7 us
    all_gather x1, blocking collectives, per_device(): second = lax.all_gather(joined, 'kv', axis=1, tiled=True)  13.2 us
    all_gather x1, blocking collectives, mix_partial(): piece = lax.all_gather(mixed, 'kv', axis=0, tiled=True)  13.1 us
    all_gather x1, blocking collectives, per_device(): lax.all_gather(norm_gain, ('kv', 'tp'), axis=1, tiled=True)  12.9 us
    dot_general x2, matrix products, feed_forward(): return jnp.dot(hidden, w_down, preferred_element_type=jnp.float32)  8.72 us
    dot_general x2, matrix products, feed_forward(): gate = jnp.dot(normed, w_gate, preferred_element_type=jnp.float32)  5.31 us
  transfers between devices with their start and end apart: 2, of which 1 were waited for; matrix products, arithmetic and copies ran while one was open for 7% of the time, Pallas kernels for 0%

profile of v1, /device:TPU:0, one launch (start us, length us, event | category | flops | bytes accessed | tf_op | source)
XLA Modules:
  0.0 143.1 jit_solution(3226332370910253282)
XLA Ops:
  0.0 14.7 %all_gather.24 = bf16[4,2048]{1,0:T(4,128)(2,1)S(1)} all-gather(bf16[4,256]{1,0:T(4,128)(2,1)} %param.18), channel_id=1, replica_groups=mesh['dp'=4,'kv'=4,'tp'=2] {'kv','tp'}, dimensions={1}, use_global_device_ids=true | all-gather | bytes 18432 | tf_op jit(solution)/shard_map/all_gather | solution.py:179
  14.7 0.1 fusion.54
  14.9 12.9 %all_gather.25 = bf16[3,2048]{1,0:T(4,128)(2,1)S(1)} all-gather(bf16[3,256]{1,0:T(4,128)(2,1)} %param.19), channel_id=1, replica_groups=mesh['dp'=4,'kv'=4,'tp'=2] {'kv','tp'}, dimensions={1}, use_global_device_ids=true | all-gather | bytes 13824 | tf_op jit(solution)/shard_map/all_gather | solution.py:180
  27.8 2.7 %fusion.10 = f32[4,704]{1,0:T(4,128)S(1)} fusion(bf16[2,2048,704]{1,2,0:T(8,128)(2,1)} %param.20, bf16[4,2048]{1,0:T(4,128)(2,1)S(1)} %all_gather.24, f32[2048]{0:T(1024)S(1)} %bitcast.121, f32[4]{0:T(128)S(1)} %add_rsqrt_fusion.2), kind=kOutput, calls=%fused_computation.10 | convolution fusion | flops 11567104 | bytes 2919440 | tf_op jit(solution)/shard_map/dot_general | solution.py:22
  30.5 4.4 %fusion.18 = f32[1,4,2048]{2,1,0:T(4,128)S(1)} fusion(bf16[2,704,2048]{2,1,0:T(8,128)(2,1)} %param.22, bf16[2,2048,704]{1,2,0:T(8,128)(2,1)} %param.21, f32[4,704]{1,0:T(4,128)S(1)} %fusion.10, bf16[4,2048]{1,0:T(4,128)(2,1)S(1)} %all_gather.24, f32[2048]{0:T(1024)S(1)} %bitcast.122, f32[4]{0:T(128)S(1)} %add_rsqrt_fusion.2), kind=kOutput, calls=%fused_computation.18 | convolution fusion | flops 23118336 | bytes 5835792 | tf_op jit(solution)/shard_map/dot_general | solution.py:25
  34.8 0.0 copy-start.6
  34.8 14.3 %all-gather.3 = f32[8,4,2048]{2,1,0:T(4,128)S(1)} all-gather(f32[1,4,2048]{2,1,0:T(4,128)S(1)} %fusion.18), channel_id=2, replica_groups=mesh['dp'=4,'kv'=4,'tp'=2] {'kv','tp'}, dimensions={0}, use_global_device_ids=true | all-gather | bytes 294912 | tf_op jit(solution)/shard_map/all_gather | solution.py:11
  49.2 0.1 fusion.51
  49.4 0.1 fusion.53
  49.5 0.0 copy-start.8
  49.5 0.0 copy-start.9
  49.5 0.0 copy-start.3
  49.5 0.0 copy-start.4
  49.5 0.6 convolution_convert_fusion.1
  50.1 0.1 reshape.198
  50.2 0.7 reshape.227
  50.9 3.2 %all-to-all-start = ((bf16[4,2,256]{2,1,0:T(2,128)(2,1)}), bf16[4,2,256]{2,1,0:T(2,128)(2,1)S(1)}, u32[]{:S(2)}, u32[]{:S(2)}) async-start(bf16[4,2,256]{2,1,0:T(2,128)(2,1)} %reshape.227), calls=%async_computation | async-start | bytes 8192 | tf_op jit(solution)/shard_map/all_to_all | solution.py:117
  54.2 0.0 copy-start.7
  54.2 2.0 %fusion.24 = f32[4,2048]{1,0:T(4,128)S(1)} fusion(bf16[64,8,16,128]{3,2,1,0:T(8,128)(2,1)} %bitcast.116, bf16[4,2048]{1,0:T(4,128)(2,1)S(1)} %fusion.53, s32[]{:T(128)S(6)} %select_n.11), kind=kOutput, calls=%fused_computation.20 | convolution fusion | flops 8388608 | bytes 2134020 | tf_op jit(solution)/shard_map/dot_general | solution.py:79
  56.2 0.1 fusion.75
  56.3 19.8 %all-reduce.2 = (bf16[4,2048]{1,0:T(4,128)(2,1)S(1)}, f32[4,64]{1,0:T(4,128)S(1)}) all-reduce(f32[4,2048]{1,0:T(4,128)S(1)} %fusion.24, f32[4,64]{1,0:T(4,128)S(1)} %fusion.75), channel_id=6, replica_groups=mesh['dp'=4,'kv'=4,'tp'=2] {'kv'}, use_global_device_ids=true, to_apply=%region_5.6.clone | all-reduce | flops 8448 | bytes 51200
  76.1 0.6 dynamic-slice
  76.7 0.7 fusion.66
  77.4 2.2 %convolution_convert_fusion = bf16[4,512]{1,0:T(4,128)(2,1)S(1)} fusion(bf16[4,2048]{1,0:T(4,128)(2,1)S(1)} %fusion.53, bf16[2048,512]{0,1:T(8,128)(2,1)} %bitcast.117), kind=kOutput, calls=%fused_computation.28 | convolution fusion | flops 8390656 | bytes 2117632 | tf_op jit(solution)/shard_map/dot_general | solution.py:112
  79.7 0.7 fusion.81
  80.4 0.1 reshape.202
  80.5 0.7 reshape.225
  81.2 0.0 all-to-all-done
  81.2 3.2 %all-to-all-start.1 = ((bf16[4,2,256]{2,1,0:T(2,128)(2,1)}), bf16[4,2,256]{2,1,0:T(2,128)(2,1)S(1)}, u32[]{:S(2)}, u32[]{:S(2)}) async-start(bf16[4,2,256]{2,1,0:T(2,128)(2,1)} %reshape.225), calls=%async_computation.1 | async-start | bytes 8192 | tf_op jit(solution)/shard_map/all_to_all | solution.py:118
  84.4 0.1 reshape.228
  84.5 0.1 copy.27
  84.6 0.0 copy-done.4
  84.6 0.1 copy.28
  84.7 1.9 %fusion.39 = f32[64,1,32]{2,1,0:T(1,128)S(1)} fusion(f32[64,128,1]{1,2,0:T(1,128)S(1)} %bitcast.118, f32[1,64,32,128]{3,2,1,0:T(8,128)S(1)} %copy-done.1, f32[64,128]{1,0:T(8,128)S(1)} %broadcast_bitcast_fusion, f32[64,32]{1,0:T(8,128)S(1)} %copy.28, f32[64]{0:T(128)S(1)} %get-tuple-element.7), kind=kOutput, calls=%fused_computation.30 | convolution fusion | flops 3932160 | bytes 1130752 | tf_op jit(solution)/shard_map/shpn,shn->shp/dot_general | solution.py:70
  86.6 0.1 copy.34
  86.7 3.3 %all-to-all-done.1 = bf16[4,2,256]{2,1,0:T(2,128)(2,1)S(1)} async-done(((bf16[4,2,256]{2,1,0:T(2,128)(2,1)}), bf16[4,2,256]{2,1,0:T(2,128)(2,1)S(1)}, u32[]{:S(2)}, u32[]{:S(2)}) %all-to-all-start.1) | async-done | bytes 4128 | tf_op jit(solution)/shard_map/all_to_all | solution.py:118
  90.0 0.1 reshape.226
  90.1 0.1 copy.30
  90.2 13.1 %all-gather.4 = bf16[4,64,32]{1,2,0:T(8,128)(2,1)S(1)} all-gather(bf16[1,64,32]{1,2,0:T(8,128)(2,1)S(1)} %fusion.70), channel_id=3, replica_groups=mesh['dp'=4,'kv'=4,'tp'=2] {'kv'}, dimensions={0}, use_global_device_ids=true | all-gather | bytes 20480 | tf_op jit(solution)/shard_map/all_gather | solution.py:139
  103.3 0.1 copy.35
  103.4 2.0 %convolution_bitcast_fusion = f32[4,512]{1,0:T(4,128)S(1)} fusion(bf16[4,64,32]{2,0,1:T(4,128)(2,1)S(1)} %copy.35, bf16[64,32,512]{2,1,0:T(8,128)(2,1)} %param.35), kind=kOutput, calls=%fused_computation.27 | convolution fusion | flops 8388608 | bytes 2121728 | tf_op jit(solution)/shard_map/dot_general | solution.py:140
  105.5 2.5 %psum.7 = f32[4,512]{1,0:T(4,128)S(1)} all-reduce(f32[4,512]{1,0:T(4,128)S(1)} %convolution_bitcast_fusion), channel_id=1, replica_groups=mesh['dp'=4,'kv'=4,'tp'=2] {'tp'}, use_global_device_ids=true, to_apply=%region_7.8 | all-reduce | flops 2048 | bytes 16384 | tf_op jit(solution)/shard_map/psum | solution.py:189
  107.9 13.2 %all_gather.29 = bf16[4,2048]{1,0:T(4,128)(2,1)S(1)} all-gather(bf16[4,512]{1,0:T(4,128)(2,1)S(1)} %add_convert_fusion), channel_id=1, replica_groups=mesh['dp'=4,'kv'=4,'tp'=2] {'kv'}, dimensions={1}, use_global_device_ids=true | all-gather | bytes 20480 | tf_op jit(solution)/shard_map/all_gather | solution.py:190
  121.2 0.1 multiply_reduce_fusion.1
  121.3 2.7 %fusion.4 = f32[4,704]{1,0:T(4,128)S(1)} fusion(bf16[2,2048,704]{1,2,0:T(8,128)(2,1)} %param.20, f32[2048]{0:T(1024)S(1)} %bitcast.119, f32[4]{0:T(128)S(1)} %add_rsqrt_fusion, bf16[4,2048]{1,0:T(4,128)(2,1)S(1)} %all_gather.29), kind=kOutput, calls=%fused_computation.4 | convolution fusion | flops 11567104 | bytes 2919440 | tf_op jit(solution)/shard_map/dot_general | solution.py:22
  124.0 4.4 %fusion.21 = f32[1,4,2048]{2,1,0:T(4,128)S(1)} fusion(bf16[2,704,2048]{2,1,0:T(8,128)(2,1)} %param.22, bf16[2,2048,704]{1,2,0:T(8,128)(2,1)} %param.21, f32[4,704]{1,0:T(4,128)S(1)} %fusion.4, f32[2048]{0:T(1024)S(1)} %bitcast.120, f32[4]{0:T(128)S(1)} %add_rsqrt_fusion, bf16[4,2048]{1,0:T(4,128)(2,1)S(1)} %all_gather.29), kind=kOutput, calls=%fused_computation.19 | convolution fusion | flops 23118336 | bytes 5835792 | tf_op jit(solution)/shard_map/dot_general | solution.py:25
  128.3 14.2 %all-gather.5 = f32[8,4,2048]{2,1,0:T(4,128)S(1)} all-gather(f32[1,4,2048]{2,1,0:T(4,128)S(1)} %fusion.21), channel_id=4, replica_groups=mesh['dp'=4,'kv'=4,'tp'=2] {'kv','tp'}, dimensions={0}, use_global_device_ids=true | all-gather | bytes 294912 | tf_op jit(solution)/shard_map/all_gather | solution.py:11
  142.6 0.6 fusion.73
  (32 shorter events, 0.3 us)
Async XLA Ops:
  0.0 49.4 %copy-start = (bf16[2048,16,32]{0,2,1:T(8,128)(2,1)S(1)}, bf16[2048,16,32]{0,2,1:T(8,128)(2,1)}, u32[]{:S(2)}) copy-start(bf16[2048,16,32]{0,2,1:T(8,128)(2,1)} %param.23) | copy-start | bytes 6291460
  34.8 21.4 %copy-start.2 = (bf16[512,64]{0,1:T(8,128)(2,1)S(1)}, bf16[512,64]{0,1:T(8,128)(2,1)}, u32[]{:S(2)}) copy-start(bf16[512,64]{0,1:T(8,128)(2,1)} %param.26) | copy-start | bytes 196612
  34.8 41.3 %copy-start.10 = (u32[32]{0:T(128)S(1)}, u32[32]{0:T(128)}, u32[]{:S(2)}) copy-start(u32[32]{0:T(128)} %constant.45) | copy-start | bytes 388
  34.8 42.5 %copy-start.5 = (bf16[4,2,8,128]{3,2,1,0:T(8,128)(2,1)S(1)}, bf16[4,2,8,128]{3,2,1,0:T(8,128)(2,1)}, u32[]{:S(2)}) copy-start(bf16[4,2,8,128]{3,2,1,0:T(8,128)(2,1)} %param.31) | copy-start | bytes 49156
  34.8 42.6 %copy-start.6 = (bf16[1,3,2,8,128]{4,3,2,1,0:T(8,128)(2,1)S(1)}, bf16[1,3,2,8,128]{4,3,2,1,0:T(8,128)(2,1)}, u32[]{:S(2)}) copy-start(bf16[1,3,2,8,128]{4,3,2,1,0:T(8,128)(2,1)} %param.33) | copy-start | bytes 36868
  49.5 30.2 %copy-start.8 = (f32[64]{0:T(128)S(1)}, f32[64]{0:T(128)}, u32[]{:S(2)}) copy-start(f32[64]{0:T(128)} %param.28) | copy-start | bytes 772
  49.5 30.2 %copy-start.9 = (f32[64]{0:T(128)S(1)}, f32[64]{0:T(128)}, u32[]{:S(2)}) copy-start(f32[64]{0:T(128)} %param.27) | copy-start | bytes 772
  49.5 35.1 %copy-start.3 = (bf16[4,64,32]{1,2,0:T(8,128)(2,1)S(1)}, bf16[4,64,32]{1,2,0:T(8,128)(2,1)}, u32[]{:S(2)}) copy-start(bf16[4,64,32]{1,2,0:T(8,128)(2,1)} %param.30) | copy-start | bytes 49156
  49.5 35.1 %copy-start.4 = (bf16[1,3,64,32]{2,3,1,0:T(8,128)(2,1)S(1)}, bf16[1,3,64,32]{2,3,1,0:T(8,128)(2,1)}, u32[]{:S(2)}) copy-start(bf16[1,3,64,32]{2,3,1,0:T(8,128)(2,1)} %param.32) | copy-start | bytes 36868
  50.1 34.6 %copy-start.1 = (f32[1,64,32,128]{3,2,1,0:T(8,128)S(1)}, f32[1,64,32,128]{3,2,1,0:T(8,128)}, u32[]{:S(2)}) copy-start(f32[1,64,32,128]{3,2,1,0:T(8,128)} %param.34) | copy-start | bytes 3145732
  50.9 30.2 %all-to-all-start = ((bf16[4,2,256]{2,1,0:T(2,128)(2,1)}), bf16[4,2,256]{2,1,0:T(2,128)(2,1)S(1)}, u32[]{:S(2)}, u32[]{:S(2)}) async-start(bf16[4,2,256]{2,1,0:T(2,128)(2,1)} %reshape.227), calls=%async_computation | async-start | bytes 8192 | tf_op jit(solution)/shard_map/all_to_all | solution.py:117
  54.2 36.0 %copy-start.7 = (f32[64]{0:T(128)S(1)}, f32[64]{0:T(128)}, u32[]{:S(2)}) copy-start(f32[64]{0:T(128)} %param.29) | copy-start | bytes 772
  81.2 8.8 %all-to-all-start.1 = ((bf16[4,2,256]{2,1,0:T(2,128)(2,1)}), bf16[4,2,256]{2,1,0:T(2,128)(2,1)S(1)}, u32[]{:S(2)}, u32[]{:S(2)}) async-start(bf16[4,2,256]{2,1,0:T(2,128)(2,1)} %reshape.225), calls=%async_computation.1 | async-start | bytes 8192 | tf_op jit(solution)/shard_map/all_to_all | solution.py:118
